TPU v7x, 32 devices: a whole 2x2x4 slice. The times are simulated.
32 devices in a mesh: sp: 16 (over z, y, x), tp: 2 (over core).
Axes of the slice: x: 2, y: 2, z: 4, core: 2. Of those that a mesh axis runs over, the one named last changes fastest.
Arguments:
- features: bfloat16 [4096, 1024], P('sp', 'tp'), may hold values from -6 to 6
- lambda_real: float32 [64, 64], P('tp'), may hold values from -4 to 0, as said below
- lambda_imag: float32 [64, 64], P('tp'), may hold values from 0.5 to 201.06177
- log_step: float32 [64], P('tp'), may hold values from -5 to -2
- input_real: float32 [64, 64, 16], P('tp'), may hold values from -2 to 2
- input_imag: float32 [64, 64, 16], P('tp'), may hold values from -2 to 2
- real_output: float32 [64, 16, 64], P('tp'), may hold values from -0.75 to 0.75
- imaginary_output: float32 [64, 16, 64], P('tp'), may hold values from -0.75 to 0.75
- skip_gain: float32 [1024], P('tp'), may hold values from -4 to 4
- value_weight: bfloat16 [1024, 2048], P('tp'), may hold values from -0.1875 to 0.1875
- gate_weight: bfloat16 [1024, 2048], P('tp'), may hold values from -0.1875 to 0.1875
- value_bias: float32 [2048], replicated, may hold values from -3 to 3
- gate_bias: float32 [2048], replicated, may hold values from -3 to 3
Outputs:
- mixed_output: bfloat16 [4096, 2048], P(('sp', 'tp'))
Inputs may be any that keep to these rules, and one draw needn't show every extreme that they name: `lambda_real`: negative.
All inputs are finite; a program needn't handle non-finite values.
Results may differ from a plain program's by a relative error of at most 0.03.
Values may be sent and summed in bfloat16 or wider, within the bound.
A program may use at most 128 MiB of HBM per device.

v0:
```python
import math

import jax
import jax.numpy as jnp
from jax import lax
from jax.sharding import PartitionSpec as P


def prefix(part, axis, combine, identity):
    place = lax.axis_index(axis)
    gathered = jax.tree.map(lambda a: lax.all_gather(a, axis), part)
    state = jax.tree.map(lambda a, e: jnp.zeros_like(a) + jnp.asarray(e, a.dtype), part, identity)

    def one(lap, state):
        return combine(
            state, jax.tree.map(lambda a: lax.dynamic_index_in_dim(a, lap, 0, False), gathered)
        )

    return lax.fori_loop(0, place, one, state)


def discretize(lambda_real, lambda_imag, log_step, input_real, input_imag):
    step_size = jnp.exp(log_step)[:, None]
    magnitude = jnp.exp(lambda_real * step_size)
    phase_arg = lambda_imag * step_size
    trans_re = magnitude * jnp.cos(phase_arg)
    trans_im = magnitude * jnp.sin(phase_arg)
    denominator = lambda_real * lambda_real + lambda_imag * lambda_imag
    num_re = trans_re - 1.0
    f_re = (num_re * lambda_real + trans_im * lambda_imag) / denominator
    f_im = (trans_im * lambda_real - num_re * lambda_imag) / denominator
    bar_re = f_re[..., None] * input_real - f_im[..., None] * input_imag
    bar_im = f_re[..., None] * input_imag + f_im[..., None] * input_real
    return (step_size, bar_re, bar_im)


def powers_flat(lambda_real, lambda_imag, step_size, first, count):
    exponent = (jnp.arange(count, dtype=jnp.int32) + first).astype(jnp.float32)[:, None]
    rate_re = (lambda_real * step_size).reshape(1, -1)
    rate_im = (lambda_imag * step_size).reshape(1, -1)
    magnitude = jnp.exp(exponent * rate_re)
    phase_arg = exponent * rate_im
    return (magnitude * jnp.cos(phase_arg), magnitude * jnp.sin(phase_arg))


def combine(earlier, later):
    a1r, a1i, b1r, b1i = earlier
    a2r, a2i, b2r, b2i = later
    return (
        a1r * a2r - a1i * a2i,
        a1r * a2i + a1i * a2r,
        a2r * b1r - a2i * b1i + b2r,
        a2r * b1i + a2i * b1r + b2i,
    )


def within_blocks(step_re, step_im, bu_re, bu_im, span):
    blocks_re = bu_re.reshape(-1, span, bu_re.shape[1])
    blocks_im = bu_im.reshape(-1, span, bu_im.shape[1])
    h_re = jnp.zeros_like(blocks_re[:, 0])
    h_im = jnp.zeros_like(blocks_im[:, 0])
    rows_re = []
    rows_im = []
    for offset in range(span):
        new_re = step_re * h_re - step_im * h_im + blocks_re[:, offset]
        new_im = step_re * h_im + step_im * h_re + blocks_im[:, offset]
        h_re, h_im = (new_re, new_im)
        rows_re.append(h_re)
        rows_im.append(h_im)
    return (jnp.stack(rows_re, axis=1), jnp.stack(rows_im, axis=1))


def block_carries(span_re, span_im, ends_re, ends_im, start_re, start_im):

    def advance(carried, ends):
        c_re, c_im = carried
        e_re, e_im = ends
        next_re = span_re * c_re - span_im * c_im + e_re
        next_im = span_re * c_im + span_im * c_re + e_im
        return ((next_re, next_im), (c_re, c_im))

    final, entering = lax.scan(advance, (start_re, start_im), (ends_re, ends_im))
    return (final, entering)


def local(
    features,
    lambda_real,
    lambda_imag,
    log_step,
    input_real,
    input_imag,
    real_output,
    imaginary_output,
    skip_gain,
    value_weight,
    gate_weight,
    value_bias,
    gate_bias,
):
    upper_limit = lax.Precision.HIGHEST
    positions = features.shape[0]
    groups = lambda_real.shape[0]
    state_width = lambda_real.shape[1]
    group_size = input_real.shape[2]
    flat_width = groups * state_width
    span = math.gcd(positions, 16)
    step_size, bar_re, bar_im = discretize(
        lambda_real, lambda_imag, log_step, input_real, input_imag
    )
    inner_re, inner_im = powers_flat(lambda_real, lambda_imag, step_size, 1, span)
    whole_re, whole_im = powers_flat(lambda_real, lambda_imag, step_size, positions, 1)
    step_re, step_im = (inner_re[0], inner_im[0])
    span_re, span_im = (inner_re[-1], inner_im[-1])
    widened = features.astype(jnp.float32)
    grouped = widened.reshape(positions, groups, group_size)
    bu_re = jnp.einsum("sgc,gpc->sgp", grouped, bar_re, precision=upper_limit).reshape(
        positions, flat_width
    )
    bu_im = jnp.einsum("sgc,gpc->sgp", grouped, bar_im, precision=upper_limit).reshape(
        positions, flat_width
    )
    local_re, local_im = within_blocks(step_re, step_im, bu_re, bu_im, span)
    ends_re, ends_im = (local_re[:, -1], local_im[:, -1])
    zero_state = jnp.zeros((flat_width,), jnp.float32)
    ones_state = jnp.ones((flat_width,), jnp.float32)
    identity = (ones_state, zero_state, zero_state, zero_state)
    final, entering = block_carries(span_re, span_im, ends_re, ends_im, zero_state, zero_state)
    enter_re = entering[0][:, None]
    enter_im = entering[1][:, None]
    signal_real = local_re + inner_re * enter_re - inner_im * enter_im
    signal_imaginary = local_im + inner_re * enter_im + inner_im * enter_re
    signal_real = signal_real.reshape(positions, flat_width)
    signal_imaginary = signal_imaginary.reshape(positions, flat_width)
    incoming = prefix((whole_re[0], whole_im[0], final[0], final[1]), "sp", combine, identity)
    h_re, h_im = (incoming[2], incoming[3])
    all_re, all_im = powers_flat(lambda_real, lambda_imag, step_size, 1, positions)
    signal_real = signal_real + all_re * h_re - all_im * h_im
    signal_imaginary = signal_imaginary + all_re * h_im + all_im * h_re
    signal_real = signal_real.reshape(positions, groups, state_width)
    signal_imaginary = signal_imaginary.reshape(positions, groups, state_width)
    mixer_response = jnp.einsum(
        "qej,eoj->qeo", signal_real, real_output, precision=upper_limit
    ) - jnp.einsum("qej,eoj->qeo", signal_imaginary, imaginary_output, precision=upper_limit)
    mixer_response = mixer_response.reshape(positions, groups * group_size) + skip_gain * widened
    activated = jax.nn.gelu(mixer_response).astype(jnp.bfloat16)
    model_width = value_weight.shape[1]
    moved = lax.all_to_all(activated, "tp", split_axis=0, concat_axis=1, tiled=True)
    full_value, full_gate = (
        lax.all_gather(value_weight, "tp", axis=0, tiled=True),
        lax.all_gather(gate_weight, "tp", axis=0, tiled=True),
    )
    pieces = lax.axis_size("tp")
    row_total = moved.shape[0]
    slice_width = value_weight.shape[0]
    blocks_act = moved.reshape(row_total, pieces, slice_width)

    def halves(weight):
        partial_value = jnp.einsum(
            "rnc,ncd->nrd",
            blocks_act,
            weight.reshape(pieces, slice_width, model_width),
            preferred_element_type=jnp.float32,
        )
        rounded = lax.optimization_barrier(partial_value.astype(jnp.bfloat16))
        return jnp.sum(rounded.astype(jnp.float32), axis=0)

    value_sum = halves(full_value)
    gate_sum = halves(full_gate)
    value_sum = value_sum + value_bias
    gate_sum = gate_sum + gate_bias
    return (value_sum * jax.nn.sigmoid(gate_sum)).astype(jnp.bfloat16)


def solution(mesh):
    in_specs = (
        P("sp", "tp"),
        P("tp", None),
        P("tp", None),
        P("tp"),
        P("tp", None, None),
        P("tp", None, None),
        P("tp", None, None),
        P("tp", None, None),
        P("tp"),
        P("tp", None),
        P("tp", None),
        P(),
        P(),
    )
    out_specs = P(("sp", "tp"), None)
    return jax.shard_map(local, mesh=mesh, in_specs=in_specs, out_specs=out_specs, check_vma=False)
```

profile of v0, /device:TPU:31, one launch (start us, length us, event | category | flops | bytes accessed | tf_op | source)
XLA Modules:
  0.0 345.8 jit_solution(2314690990529979079)
XLA Ops:
  9.6 2.4 convolution_bitcast_fusion.1
  14.4 5.8 %copy.90 = f32[256,32,64]{2,1,0:T(8,128)} copy(f32[256,32,64]{0,2,1:T(8,128)} %convolution_bitcast_fusion.1) | data formatting | bytes 4194304 | tf_op jit(solution)/shard_map/sgc,gpc->sgp/transpose | solution.py:117
  20.1 4.9 %reshape_reshape.6 = f32[16,16,2048]{2,1,0:T(8,128)} reshape(f32[256,32,64]{2,1,0:T(8,128)} %copy.90) | data formatting | bytes 4194304 | tf_op jit(solution)/shard_map/reshape;reshape | solution.py:58
  25.0 9.8 %fusion.35 = (f32[16,1,2048]{2,1,0:T(1,128)}, f32[16,1,2048]{2,1,0:T(1,128)S(1)}, f32[16,1,2048]{2,1,0:T(1,128)}, f32[16,1,2048]{2,1,0:T(1,128)}, f32[16,1,2048]...) fusion(f32[16,16,2048]{2,1,0:T(8,128)} %reshape_reshape.6), kind=kLoop, calls=%fused_computation.170 | loop fusion | bytes 4194304 | tf_op jit(solution)/shard_map/slice | solution.py:65
  34.8 4.5 %copy.92 = f32[256,32,64]{2,1,0:T(8,128)} copy(f32[256,32,64]{0,2,1:T(8,128)S(1)} %convolution_bitcast_fusion) | data formatting | bytes 4194304 | tf_op jit(solution)/shard_map/sgc,gpc->sgp/transpose | solution.py:120
  39.3 3.6 %reshape_reshape.7 = f32[16,16,2048]{2,1,0:T(8,128)S(1)} reshape(f32[256,32,64]{2,1,0:T(8,128)} %copy.92) | data formatting | bytes 4194304 | tf_op jit(solution)/shard_map/reshape;reshape | solution.py:59
  43.0 1.6 fusion.34
  48.4 48.8 %while.33 = (s32[]{:T(128)}, f32[2048]{0:T(1024)S(1)}, f32[2048]{0:T(1024)S(1)}, f32[16,2048]{1,0:T(8,128)}, f32[16,2048]{1,0:T(8,128)}, /*index=5*/f32[2048]{0:...) while((s32[]{:T(128)}, f32[2048]{0:T(1024)S(1)}, ...), condition=%wide.region_1.2_spmd.clone, body=%wide.region_0.1_spmd.clone.sunk | while | flops 20483 | bytes 180355 | solution.py:82
  48.5 1.6 dynamic_update_slice.11
  73.0 1.5 dynamic_update_slice.11
  76.0 1.5 dynamic_update_slice.11
  79.0 1.5 dynamic_update_slice.11
  82.1 1.5 dynamic_update_slice.11
  85.1 1.5 dynamic_update_slice.11
  88.2 1.5 dynamic_update_slice.11
  91.2 1.5 dynamic_update_slice.11
  97.2 29.1 %all-gather = f32[32768]{0:T(1024)S(1)} all-gather(f32[2048]{0:T(1024)S(1)} %get-tuple-element.127), channel_id=2, replica_groups=mesh['sp'=16,'tp'=2] {'sp'}, dimensions={0}, use_global_device_ids=true | all-gather | bytes 139264 | tf_op jit(solution)/shard_map/all_gather | solution.py:11
  126.4 31.3 %all-gather.1 = f32[32768]{0:T(1024)S(1)} all-gather(f32[2048]{0:T(1024)S(1)} %get-tuple-element.128), channel_id=3, replica_groups=mesh['sp'=16,'tp'=2] {'sp'}, dimensions={0}, use_global_device_ids=true | all-gather | bytes 139264 | tf_op jit(solution)/shard_map/all_gather | solution.py:11
  157.8 29.5 %all-gather.3 = f32[16,1,2048]{2,1,0:T(1,128)S(1)} all-gather(f32[1,1,2048]{2,1,0:T(1,128)S(1)} %reshape.5975), channel_id=1, replica_groups=mesh['sp'=16,'tp'=2] {'sp'}, dimensions={0}, use_global_device_ids=true | all-gather | bytes 139264 | tf_op jit(solution)/shard_map/all_gather | solution.py:11
  188.1 30.6 %all-gather.2 = f32[16,1,2048]{2,1,0:T(1,128)S(1)} all-gather(f32[1,1,2048]{2,1,0:T(1,128)S(1)} %reshape.5973), channel_id=1, replica_groups=mesh['sp'=16,'tp'=2] {'sp'}, dimensions={0}, use_global_device_ids=true | all-gather | bytes 139264 | tf_op jit(solution)/shard_map/all_gather | solution.py:11
  219.4 14.7 %while.32 = (s32[]{:T(128)}, f32[2048]{0:T(1024)S(1)}, f32[2048]{0:T(1024)S(1)}, s32[]{:T(128)}, f32[16,2048]{1,0:T(8,128)}, /*index=5*/f32[16,2048]{1,0:T(8,128...) while((s32[]{:T(128)}, f32[2048]{0:T(1024)S(1)}, ...), condition=%wide.region_3.4_spmd, body=%wide.region_2.3_spmd.sunk | while | flops 16389 | bytes 131223 | solution.py:19
  248.3 2.8 multiply_subtract_fusion.1
  251.1 2.5 copy.126
  253.6 4.9 %add.1212 = f32[256,32,64]{2,1,0:T(8,128)} reshape(f32[16,16,2048]{2,1,0:T(8,128)} %copy.126) | data formatting | bytes 4194304 | tf_op jit(solution)/shard_map/add | solution.py:132
  258.5 2.5 copy.124
  261.1 4.9 %sub.375 = f32[256,32,64]{2,1,0:T(8,128)} reshape(f32[16,16,2048]{2,1,0:T(8,128)} %copy.124) | data formatting | bytes 4194304 | tf_op jit(solution)/shard_map/sub | solution.py:131
  266.0 19.2 %multiply_subtract_fusion = (f32[256,32,64]{2,1,0:T(8,128)S(1)}, f32[256,32,64]{2,1,0:T(8,128)S(1)}) fusion(f32[256,32,64]{2,1,0:T(8,128)} %sub.375, f32[32,64]{1,0:T(8,128)S(1)} %mul.2004, f32[32,64]{1,0:T(8,128)S(1)} %mul.2000, f32[32,64]{1,0:T(8,128)S(1)} %copy-done.52, f32[32,64]{1,0:T(8,128)S(1)} %copy-done.54, f32[256]{0:T(256)S(1)} %add_convert_fusion, ...), kind=kLoop, calls=%fused_computation.21 | loop fusion | flops 6291456 | bytes 8422400 | tf_op jit(solution)/shard_map/sub | solution.py:138
  285.2 6.1 %fusion.2 = f32[32,256,16]{1,2,0:T(8,128)S(1)} fusion(f32[32,16,64]{2,1,0:T(8,128)S(1)} %copy-done, f32[256,32,64]{2,1,0:T(8,128)S(1)} %get-tuple-element.313), kind=kOutput, calls=%fused_computation.16 | convolution fusion | flops 100663296 | bytes 2752512 | tf_op jit(solution)/shard_map/qej,eoj->qeo/dot_general | solution.py:144
  291.3 6.1 %fusion.6 = f32[32,256,16]{1,2,0:T(8,128)S(1)} fusion(f32[32,256,16]{1,2,0:T(8,128)S(1)} %fusion.2, f32[32,16,64]{2,1,0:T(8,128)S(1)} %copy-done.50, f32[256,32,64]{2,1,0:T(8,128)S(1)} %get-tuple-element.312), kind=kOutput, calls=%fused_computation.31 | convolution fusion | flops 100794368 | bytes 3276800 | tf_op jit(solution)/shard_map/qej,eoj->qeo/dot_general | solution.py:142
  297.9 32.7 %all_to_all.16 = bf16[2,128,512]{2,1,0:T(8,128)(2,1)S(1)} all-to-all(bf16[2,128,512]{2,1,0:T(8,128)(2,1)S(1)} %bitcast.277), channel_id=1, replica_groups=mesh['sp'=16,'tp'=2] {'tp'}, dimensions={0} | all-to-all | bytes 524288 | tf_op jit(solution)/shard_map/all_to_all | solution.py:148
  330.6 2.9 convolution_convert_fusion.1
  333.7 2.9 convolution_convert_fusion
  (312 shorter events, 77.1 us)
Async XLA Ops:
  6.5 278.6 %copy-start = (f32[32,16,64]{2,1,0:T(8,128)S(1)}, f32[32,16,64]{2,1,0:T(8,128)}, u32[]{:S(2)}) copy-start(f32[32,16,64]{2,1,0:T(8,128)} %param.24) | copy-start | bytes 393220
  6.6 324.0 %all-gather.7.cloned.1.call-start = ((), (), s32[]{:S(2)}) async-start(), calls=%async_computation.1 | async-start | bytes 6291456 | tf_op jit(solution)/shard_map/all_gather | solution.py:150
  7.3 326.4 %all-gather.9.cloned.1.call-start = ((), (), s32[]{:S(2)}) async-start(), calls=%async_computation.2 | async-start | bytes 6291456 | tf_op jit(solution)/shard_map/all_gather | solution.py:151
  9.6 3.4 copy-start.53
  9.6 4.1 %copy-start.51 = (f32[32,64]{1,0:T(8,128)}, f32[32,64]{1,0:T(8,128)S(1)}, u32[]{:S(2)}) copy-start(f32[32,64]{1,0:T(8,128)S(1)} %get-tuple-element.318) | copy-start | bytes 24580
  43.0 3.2 copy-start.30
  43.0 3.2 copy-start.34
  43.0 3.1 copy-start.40
  43.0 3.5 %copy-start.15 = (f32[16,1,2048]{2,1,0:T(1,128)S(1)}, f32[16,1,2048]{2,1,0:T(1,128)}, u32[]{:S(2)}) copy-start(f32[16,1,2048]{2,1,0:T(1,128)} %get-tuple-element.281) | copy-start | bytes 393220
  43.0 3.5 %copy-start.19 = (f32[16,1,2048]{2,1,0:T(1,128)S(1)}, f32[16,1,2048]{2,1,0:T(1,128)}, u32[]{:S(2)}) copy-start(f32[16,1,2048]{2,1,0:T(1,128)} %get-tuple-element.283) | copy-start | bytes 393220
  43.0 3.5 %copy-start.23 = (f32[16,1,2048]{2,1,0:T(1,128)S(1)}, f32[16,1,2048]{2,1,0:T(1,128)}, u32[]{:S(2)}) copy-start(f32[16,1,2048]{2,1,0:T(1,128)} %get-tuple-element.284) | copy-start | bytes 393220
  47.6 110.1 %copy-start.58 = (f32[32,64]{1,0:T(8,128)S(1)}, f32[32,64]{1,0:T(8,128)}, u32[]{:S(2)}) copy-start(f32[32,64]{1,0:T(8,128)} %get-tuple-element.314) | copy-start | bytes 24580
  48.2 139.8 %copy-start.57 = (f32[32,64]{1,0:T(8,128)S(1)}, f32[32,64]{1,0:T(8,128)}, u32[]{:S(2)}) copy-start(f32[32,64]{1,0:T(8,128)} %get-tuple-element.315) | copy-start | bytes 24580
  48.4 185.7 %copy-start.41 = (f32[16,1,2048]{2,1,0:T(1,128)S(1)}, f32[16,1,2048]{2,1,0:T(1,128)}, u32[]{:S(2)}) copy-start(f32[16,1,2048]{2,1,0:T(1,128)} %get-tuple-element.287) | copy-start | bytes 393220
  48.4 186.6 %copy-start.35 = (f32[16,1,2048]{2,1,0:T(1,128)S(1)}, f32[16,1,2048]{2,1,0:T(1,128)}, u32[]{:S(2)}) copy-start(f32[16,1,2048]{2,1,0:T(1,128)} %get-tuple-element.286) | copy-start | bytes 393220
  48.4 186.5 %copy-start.39 = (f32[16,1,2048]{2,1,0:T(1,128)S(1)}, f32[16,1,2048]{2,1,0:T(1,128)}, u32[]{:S(2)}) copy-start(f32[16,1,2048]{2,1,0:T(1,128)} %copy-done.38) | copy-start | bytes 393220
  126.3 109.5 %copy-start.31 = (f32[16,1,2048]{2,1,0:T(1,128)S(1)}, f32[16,1,2048]{2,1,0:T(1,128)}, u32[]{:S(2)}) copy-start(f32[16,1,2048]{2,1,0:T(1,128)} %get-tuple-element.285) | copy-start | bytes 393220
  126.4 109.5 %copy-start.37 = (f32[16,1,2048]{2,1,0:T(1,128)S(1)}, f32[16,1,2048]{2,1,0:T(1,128)}, u32[]{:S(2)}) copy-start(f32[16,1,2048]{2,1,0:T(1,128)} %copy-done.36) | copy-start | bytes 393220
  219.4 17.3 %copy-start.24 = (f32[16,1,2048]{2,1,0:T(1,128)S(1)}, f32[16,1,2048]{2,1,0:T(1,128)}, u32[]{:S(2)}) copy-start(f32[16,1,2048]{2,1,0:T(1,128)} %get-tuple-element.284) | copy-start | bytes 393220
  219.4 17.3 %copy-start.33 = (f32[16,1,2048]{2,1,0:T(1,128)S(1)}, f32[16,1,2048]{2,1,0:T(1,128)}, u32[]{:S(2)}) copy-start(f32[16,1,2048]{2,1,0:T(1,128)} %copy-done.32) | copy-start | bytes 393220
  234.2 3.4 copy-start.20
  234.2 3.4 copy-start.26
  244.2 3.3 copy-start.28
  244.3 4.0 %copy-start.47 = (f32[16,2048]{1,0:T(8,128)S(1)}, f32[16,2048]{1,0:T(8,128)}, u32[]{:S(2)}) copy-start(f32[16,2048]{1,0:T(8,128)} %copy-done.46) | copy-start | bytes 393220
  244.3 4.0 %copy-start.49 = (f32[16,2048]{1,0:T(8,128)S(1)}, f32[16,2048]{1,0:T(8,128)}, u32[]{:S(2)}) copy-start(f32[16,2048]{1,0:T(8,128)} %copy-done.48) | copy-start | bytes 393220
  245.1 3.2 copy-start.55
  245.1 3.2 copy-start.56
  261.0 4.9 %copy-start.52 = (f32[32,64]{1,0:T(8,128)S(1)}, f32[32,64]{1,0:T(8,128)}, u32[]{:S(2)}) copy-start(f32[32,64]{1,0:T(8,128)} %copy-done.51) | copy-start | bytes 24580
  261.1 4.9 %copy-start.54 = (f32[32,64]{1,0:T(8,128)S(1)}, f32[32,64]{1,0:T(8,128)}, u32[]{:S(2)}) copy-start(f32[32,64]{1,0:T(8,128)} %copy-done.53) | copy-start | bytes 24580
  285.2 6.1 %copy-start.50 = (f32[32,16,64]{2,1,0:T(8,128)S(1)}, f32[32,16,64]{2,1,0:T(8,128)}, u32[]{:S(2)}) copy-start(f32[32,16,64]{2,1,0:T(8,128)} %param.23) | copy-start | bytes 393220
  291.3 6.3 %copy-start.45 = (bf16[256,512]{1,0:T(8,128)(2,1)S(1)}, bf16[256,512]{1,0:T(8,128)(2,1)}, u32[]{:S(2)}) copy-start(bf16[256,512]{1,0:T(8,128)(2,1)} %param.17) | copy-start | bytes 786436
  291.3 6.3 %copy-start.65 = (f32[512]{0:T(512)S(1)}, f32[512]{0:T(512)}, u32[]{:S(2)}) copy-start(f32[512]{0:T(512)} %param.25) | copy-start | bytes 6148
  (38 other events, 86.9 us)
Sparse Core Ops, SparseCore 0:
  8.9 15.2 all-gather.6
  25.8 14.8 all-gather.8
where the time goes:
time: 351 us; the launch traced here: 346 us
  blocking collectives  153 us (44%)
  local copies, waits for them, and re-layouts  112 us (32%)
  other arithmetic  42 us (12%)
  matrix products  21.4 us (6%)
  between operations  14.7 us (4%)
    all_gather x4, blocking collectives, prefix(): gathered = jax.tree.map(lambda a: lax.all_gather(a, axis), part)  121 us
    dynamic_update_slice x32, local copies, waits for them, and re-layouts, block_carries(): lax.scan(advance, (start_re, start_im), (ends_re, ends_im))  47.9 us
    all_to_all x1, blocking collectives, local(): lax.all_to_all(activated, 'tp', split_axis=0, concat_axis=1, tiled=True)  32.7 us
    sub x1, other arithmetic, local(): signal_real = signal_real + all_re * h_re - all_im * h_im  19.2 us
    dynamic_slice x30, local copies, waits for them, and re-layouts, one(): lax.dynamic_index_in_dim(a, lap, 0, False)  13.7 us
    unnamed x17, other arithmetic  12.3 us
    slice x1, local copies, waits for them, and re-layouts, within_blocks(): new_re = step_re * h_re - step_im * h_im + blocks_re[:, offset]  9.78 us
    sub x2, local copies, waits for them, and re-layouts, local(): signal_real = local_re + inner_re * enter_re - inner_im * enter_im  7.42 us
  transfers between devices with their start and end apart: 2, of which 0 were waited for; matrix products, arithmetic and copies ran while one was open for 49% of the time, Pallas kernels for 0%

commit v1 on v0

v1 whole, which is shorter than its diff:
```python
import functools

import jax
import jax.numpy as jnp
from jax import lax
from jax.experimental import pallas as pl
from jax.experimental.pallas import tpu as pltpu
from jax.sharding import PartitionSpec as P

MESH = pl.DeviceIdType.MESH
F32 = jnp.float32
BF16 = jnp.bfloat16


def iota(shape, dim):
    return lax.broadcasted_iota(jnp.int32, shape, dim)


def cmul(ar, ai, br, bi):
    return ar * br - ai * bi, ar * bi + ai * br


def nt_dot(left, right):
    return lax.dot_general(left, right, (((1,), (1,)), ((), ())), preferred_element_type=F32)


def kernel(nsp, ntp, dims, *refs):
    rows, groups, state, size, width = dims
    (x_h, lr_h, li_h, ls_h, br_h, bi_h, cr_h, ci_h, sk_h, vw_h, gw_h, vb_h, gb_h, out_ref,
     x_v, lr_v, li_v, ls_v, br_v, bi_v, cr_v, ci_v, sk_v, vw_v, gw_v, vb_v, gb_v,
     xp_v, zr_v, zi_v, zcat_v, wcat_v, crm_v, cim_v, resp_v, act_v,
     hx_v, fin_v, a_all_v, msg_v, recv_v, h_v, part_v, inbox_v,
     in_sem, send_sem, recv_sem, psend_sem, precv_sem) = refs
    me = lax.axis_index("sp")
    core = lax.axis_index("tp")
    gpb = 128 // size
    lanes = gpb * state
    blocks = groups // gpb
    chunks = 16
    length = rows // chunks
    own_rows = rows // ntp

    hbm = (ls_h, lr_h, li_h, x_h, br_h, bi_h, cr_h, ci_h, sk_h, vb_h, gb_h, vw_h, gw_h)
    vmem = (ls_v, lr_v, li_v, x_v, br_v, bi_v, cr_v, ci_v, sk_v, vb_v, gb_v, vw_v, gw_v)
    copies = [pltpu.make_async_copy(s, d, in_sem.at[i]) for i, (s, d) in enumerate(zip(hbm, vmem))]
    for c in copies:
        c.start()

    barrier = pltpu.get_barrier_semaphore()
    for k in range(1, ntp):
        pl.semaphore_signal(barrier, inc=1, device_id=(me, lax.rem(core + k, ntp)), device_id_type=MESH)

    @pl.loop(1, nsp)
    def _(k):
        pl.semaphore_signal(barrier, inc=1, device_id=(lax.rem(me + k, nsp), core), device_id_type=MESH)

    for c in copies[:3]:
        c.wait()
    eye = iota((groups, groups), 0) == iota((groups, groups), 1)
    step = jnp.exp(jnp.sum(jnp.where(eye, ls_v[...], 0.0), axis=1, keepdims=True))
    lam_r, lam_i = lr_v[...], li_v[...]
    mag = jnp.exp(lam_r * step)
    phase = lam_i * step
    t_r, t_i = mag * jnp.cos(phase), mag * jnp.sin(phase)
    den = lam_r * lam_r + lam_i * lam_i
    n_r = t_r - 1.0
    f_r = (n_r * lam_r + t_i * lam_i) / den
    f_i = (t_i * lam_r - n_r * lam_i) / den

    per = 128 // state
    row8, lane8 = iota((gpb, 128), 0), iota((gpb, 128), 1)

    def flat(value, b):
        sub = value[b * gpb:(b + 1) * gpb]
        dup = jnp.concatenate([sub] * per, axis=1)
        return jnp.concatenate(
            [jnp.sum(jnp.where(row8 == per * j + lane8 // state, dup, 0.0), axis=0, keepdims=True)
             for j in range(gpb // per)], axis=1)

    r0, r1 = iota((rows, rows), 0), iota((rows, rows), 1)
    shuffle = jnp.where(r1 == (r0 % chunks) * length + r0 // chunks, 1.0, 0.0).astype(BF16)
    copies[3].wait()
    xp_v[...] = jnp.dot(shuffle, x_v[...], preferred_element_type=F32).astype(BF16)

    spread = jnp.where(iota((size, 128), 1) % size == iota((size, 128), 0), 1.0, 0.0).astype(BF16)
    b_mask = iota((lanes, 128), 0) // state == iota((lanes, 128), 1) // size
    copies[4].wait()
    copies[5].wait()
    crow = iota((chunks, lanes), 0)

    def shift(value, s):
        return jnp.where(crow >= s, pltpu.roll(value, s, 0), 0.0)

    powers = []
    for b in range(blocks):
        xb = xp_v[:, b * 128:(b + 1) * 128]

        def inject(ref):
            flat_b = ref[b * gpb:(b + 1) * gpb].reshape(lanes, size).astype(BF16)
            wide = jnp.dot(flat_b, spread, preferred_element_type=F32)
            return nt_dot(xb, jnp.where(b_mask, wide, 0.0).astype(BF16))

        zr_v[b] = inject(br_v)
        zi_v[b] = inject(bi_v)
        a1r, a1i = flat(t_r, b), flat(t_i, b)
        ar, ai = jnp.broadcast_to(a1r, (chunks, lanes)), jnp.broadcast_to(a1i, (chunks, lanes))
        z_r = z_i = None
        for o in range(length):
            here = pl.ds(o * chunks, chunks)
            if o == 0:
                z_r, z_i = zr_v[b, here, :], zi_v[b, here, :]
            else:
                p_r, p_i = cmul(ar, ai, z_r, z_i)
                z_r, z_i = p_r + zr_v[b, here, :], p_i + zi_v[b, here, :]
                zr_v[b, here, :] = z_r
                zi_v[b, here, :] = z_i
        qr, qi = ar, ai
        s = 1
        while s < length:
            qr, qi = cmul(qr, qi, qr, qi)
            s *= 2
        pw_r, pw_i = jnp.ones_like(qr), jnp.zeros_like(qr)
        s = 1
        while s < chunks:
            m_r, m_i = cmul(qr, qi, shift(z_r, s), shift(z_i, s))
            z_r, z_i = z_r + m_r, z_i + m_i
            bit = (crow // s) % 2 == 1
            pw_r, pw_i = cmul(pw_r, pw_i, jnp.where(bit, qr, 1.0), jnp.where(bit, qi, 0.0))
            qr, qi = cmul(qr, qi, qr, qi)
            s *= 2
        hx_v[0, b], hx_v[1, b] = shift(z_r, 1), shift(z_i, 1)
        fin_v[b:b + 1] = z_r[chunks - 1:]
        fin_v[blocks + b:blocks + b + 1] = z_i[chunks - 1:]
        a_all_v[b:b + 1] = qr[:1]
        a_all_v[blocks + b:blocks + b + 1] = qi[:1]
        hx_v[2, b], hx_v[3, b] = pw_r, pw_i
    msg_v[...] = fin_v[...].astype(BF16)

    pl.semaphore_wait(barrier, nsp - 1 + ntp - 1)

    def outgoing(d):
        return pltpu.make_async_remote_copy(
            src_ref=msg_v, dst_ref=recv_v.at[me], send_sem=send_sem.at[d], recv_sem=recv_sem.at[me],
            device_id=(d, core), device_id_type=MESH)

    @pl.loop(me + 1, nsp)
    def _(d):
        outgoing(nsp + me - d).start()

    copies[6].wait()
    copies[7].wait()
    copies[8].wait()
    c_mask = iota((128, lanes), 0) // size == iota((128, lanes), 1) // state
    for b in range(blocks):
        a1r, a1i = flat(t_r, b), flat(t_i, b)
        ar, ai = jnp.broadcast_to(a1r, (chunks, lanes)), jnp.broadcast_to(a1i, (chunks, lanes))
        w_r, w_i = hx_v[0, b], hx_v[1, b]
        p_r, p_i = hx_v[2, b], hx_v[3, b]
        for o in range(length):
            here = pl.ds(o * chunks, chunks)
            w_r, w_i = cmul(ar, ai, w_r, w_i)
            p_r, p_i = cmul(ar, ai, p_r, p_i)
            zcat_v[here, :lanes] = (zr_v[b, here, :] + w_r).astype(BF16)
            zcat_v[here, lanes:] = (zi_v[b, here, :] + w_i).astype(BF16)
            wcat_v[b, here, :lanes] = p_r.astype(BF16)
            wcat_v[b, here, lanes:] = p_i.astype(BF16)
        gains_r, gains_i = [], []
        for g in range(b * gpb, (b + 1) * gpb):
            g_r, g_i = cmul(cr_v[g], ci_v[g], f_r[g:g + 1], f_i[g:g + 1])
            gains_r.append(g_r)
            gains_i.append(g_i)

        def diagonal(parts):
            tall = jnp.concatenate(parts, axis=0)
            wide = jnp.concatenate([tall] * gpb, axis=1)
            return jnp.where(c_mask, wide, 0.0)

        m_r, m_i = diagonal(gains_r), diagonal(gains_i)
        crm_v[b], cim_v[b] = m_r, m_i
        mats = jnp.concatenate([m_r.astype(BF16), (-m_i).astype(BF16)], axis=1)
        col = pl.ds(b * 128, 128)
        resp_v[:, col] = nt_dot(zcat_v[...], mats) + sk_v[:, col] * xp_v[:, col].astype(F32)

    A_r, A_i = a_all_v[:blocks], a_all_v[blocks:]
    zero = jnp.zeros((blocks, lanes), F32)

    def horner(d, h):
        pltpu.make_async_remote_copy(
            src_ref=msg_v, dst_ref=recv_v.at[d], send_sem=send_sem.at[d], recv_sem=recv_sem.at[d],
            device_id=(d, core), device_id_type=MESH).wait_recv()
        got = recv_v[d].astype(F32)
        n_r, n_i = cmul(A_r, A_i, h[0], h[1])
        return n_r + got[:blocks], n_i + got[blocks:]

    h_r, h_i = lax.fori_loop(0, me, horner, (zero, zero))
    h_v[:blocks] = h_r
    h_v[blocks:] = h_i

    for b in range(blocks):
        k_r, k_i = cmul(crm_v[b], cim_v[b], h_v[b:b + 1], h_v[blocks + b:blocks + b + 1])
        mats = jnp.concatenate([k_r.astype(BF16), (-k_i).astype(BF16)], axis=1)
        col = pl.ds(b * 128, 128)
        total = resp_v[:, col] + nt_dot(wcat_v[b], mats)
        act_v[:, col] = jax.nn.gelu(total).astype(BF16)

    back = jnp.where(r1 == (r0 % length) * chunks + r0 // length, 1.0, 0.0).astype(BF16)
    act = jnp.dot(back, act_v[...], preferred_element_type=F32).astype(BF16)

    for c in copies[9:]:
        c.wait()
    piece = inbox_v.shape[-1]
    pieces = width // piece

    def exchange(j, k):
        to = lax.rem(core + k, ntp)
        return pltpu.make_async_remote_copy(
            src_ref=part_v.at[j, to], dst_ref=inbox_v.at[j, k - 1],
            send_sem=psend_sem.at[j, k - 1], recv_sem=precv_sem.at[j, k - 1],
            device_id=(me, to), device_id_type=MESH)

    for j in range(pieces):
        col = pl.ds(j * piece, piece)
        for which, weight in enumerate((vw_v, gw_v)):
            part = jnp.dot(act, weight[:, col], preferred_element_type=F32).astype(BF16)
            for i in range(ntp):
                part_v[j, i, which] = part[i * own_rows:(i + 1) * own_rows]
        for k in range(1, ntp):
            exchange(j, k).start()
    for j in range(pieces):
        col = pl.ds(j * piece, piece)
        for k in range(1, ntp):
            exchange(j, k).wait_recv()
        sums = []
        for which, bias in enumerate((vb_v, gb_v)):
            total = part_v[j, core, which].astype(F32)
            for k in range(1, ntp):
                total = total + inbox_v[j, k - 1, which].astype(F32)
            sums.append(total + bias[:, col])
        out_ref[:, col] = (sums[0] * jax.nn.sigmoid(sums[1])).astype(BF16)
    for j in range(pieces):
        for k in range(1, ntp):
            exchange(j, k).wait_send()

    @pl.loop(me + 1, nsp)
    def _(d):
        outgoing(nsp + me - d).wait_send()


def local(nsp, ntp, features, lambda_real, lambda_imag, log_step, input_real, input_imag, real_output,
          imaginary_output, skip_gain, value_weight, gate_weight, value_bias, gate_bias):
    rows, channels = features.shape
    groups, state = lambda_real.shape
    size = input_real.shape[2]
    width = value_weight.shape[1]
    gpb = 128 // size
    lanes, blocks, chunks = gpb * state, groups // gpb, 16
    piece = min(512, width)
    args = (features, lambda_real, lambda_imag, log_step[None], input_real, input_imag, real_output,
            imaginary_output, skip_gain[None], value_weight, gate_weight, value_bias[None], gate_bias[None])
    scratch = [pltpu.VMEM(a.shape, a.dtype) for a in args]
    scratch += [
        pltpu.VMEM((rows, channels), BF16),
        pltpu.VMEM((blocks, rows, lanes), F32),
        pltpu.VMEM((blocks, rows, lanes), F32),
        pltpu.VMEM((rows, 2 * lanes), BF16),
        pltpu.VMEM((blocks, rows, 2 * lanes), BF16),
        pltpu.VMEM((blocks, 128, lanes), F32),
        pltpu.VMEM((blocks, 128, lanes), F32),
        pltpu.VMEM((rows, channels), F32),
        pltpu.VMEM((rows, channels), BF16),
        pltpu.VMEM((4, blocks, chunks, lanes), F32),
        pltpu.VMEM((2 * blocks, lanes), F32),
        pltpu.VMEM((2 * blocks, lanes), F32),
        pltpu.VMEM((2 * blocks, lanes), BF16),
        pltpu.VMEM((nsp, 2 * blocks, lanes), BF16),
        pltpu.VMEM((2 * blocks, lanes), F32),
        pltpu.VMEM((width // piece, ntp, 2, rows // ntp, piece), BF16),
        pltpu.VMEM((width // piece, ntp - 1, 2, rows // ntp, piece), BF16),
        pltpu.SemaphoreType.DMA((len(args),)),
        pltpu.SemaphoreType.DMA((nsp,)),
        pltpu.SemaphoreType.DMA((nsp,)),
        pltpu.SemaphoreType.DMA((width // piece, ntp - 1)),
        pltpu.SemaphoreType.DMA((width // piece, ntp - 1)),
    ]
    return pl.pallas_call(
        functools.partial(kernel, nsp, ntp, (rows, groups, state, size, width)),
        out_shape=jax.ShapeDtypeStruct((rows // ntp, width), BF16),
        in_specs=[pl.BlockSpec(memory_space=pl.ANY)] * len(args),
        out_specs=pl.BlockSpec(memory_space=pltpu.VMEM),
        scratch_shapes=scratch,
        compiler_params=pltpu.CompilerParams(
            collective_id=0, has_side_effects=True, vmem_limit_bytes=60 * 1024 * 1024),
        name="mixer",
    )(*args)


def solution(mesh):
    in_specs = (
        P("sp", "tp"),
        P("tp", None),
        P("tp", None),
        P("tp"),
        P("tp", None, None),
        P("tp", None, None),
        P("tp", None, None),
        P("tp", None, None),
        P("tp"),
        P("tp", None),
        P("tp", None),
        P(),
        P(),
    )
    out_specs = P(("sp", "tp"), None)
    body = functools.partial(local, mesh.shape["sp"], mesh.shape["tp"])
    return jax.shard_map(body, mesh=mesh, in_specs=in_specs, out_specs=out_specs, check_vma=False)
```

time: 351 us -> 22.7 us (0.06)
  the two profiles are of different devices: /device:TPU:31 before, /device:TPU:17 now
where the time goes in v1:
time: 22.7 us; the launch traced here: 22.5 us
  Pallas kernels  15.9 us (70%)
  local copies, waits for them, and re-layouts  6.52 us (29%)
    pallas_call x1, Pallas kernels, local(): pl.pallas_call(functools.partial(kernel, nsp, ntp, (rows, groups, state,...  15.9 us
    unnamed x3, local copies, waits for them, and re-layouts  6.52 us

profile of v1, /device:TPU:17, one launch (start us, length us, event | category | flops | bytes accessed | tf_op | source)
XLA Modules:
  0.0 22.5 jit_solution(4806690220589379355)
XLA Ops:
  0.0 2.3 %copy.14.refs_4_ = f32[32,64,16]{2,1,0:T(8,128)} copy(f32[32,64,16]{1,2,0:T(8,128)} %param.17) | data formatting | bytes 262144 | tf_op args[4]
  2.3 2.3 %copy.15.refs_5_ = f32[32,64,16]{2,1,0:T(8,128)} copy(f32[32,64,16]{1,2,0:T(8,128)} %param.18) | data formatting | bytes 262144 | tf_op args[5]
  4.6 15.9 %mixer.1 = bf16[128,2048]{1,0:T(8,128)(2,1)} custom-call(bf16[256,512]{1,0:T(8,128)(2,1)} %refs_0_.1, f32[32,64]{1,0:T(8,128)} %refs_1_.1, f32[32,64]{1,0:T(8,128)} %refs_2_.1, f32[1,32]{1,0:T(1,128)} %bitcast.7, f32[32,64,16]{2,1,0:T(8,128)} %copy.14.refs_4_, f32[32,64,16]{2,1,0:T(8,128)} %copy.15.refs_5_, f32[32,16,64]{2,1,0:T(8,128)} %refs_6_.1, ...), custom_call_target="tpu_custom_call" | custom-call | tf_op jit(solution)/shard_map/mixer/pallas_call | solution.py:285
  20.6 1.9 %copy.17 = bf16[128,2048]{1,0:T(8,128)(2,1)} copy(bf16[128,2048]{1,0:T(8,128)(2,1)} %mixer.1) | data formatting | bytes 1048576

commit v2 on v1

--- a/solution.py
+++ b/solution.py
@@ -82,8 +82,12 @@
     copies[3].wait()
     xp_v[...] = jnp.dot(shuffle, x_v[...], preferred_element_type=F32).astype(BF16)
 
-    spread = jnp.where(iota((size, 128), 1) % size == iota((size, 128), 0), 1.0, 0.0).astype(BF16)
-    b_mask = iota((lanes, 128), 0) // state == iota((lanes, 128), 1) // size
+
+    c_mask = iota((128, lanes), 0) // size == iota((128, lanes), 1) // state
+
+    def diagonal(tall):
+        return jnp.where(c_mask, jnp.concatenate([tall] * gpb, axis=1), 0.0)
+
     copies[4].wait()
     copies[5].wait()
     crow = iota((chunks, lanes), 0)
@@ -91,14 +95,12 @@
     def shift(value, s):
         return jnp.where(crow >= s, pltpu.roll(value, s, 0), 0.0)
 
-    powers = []
     for b in range(blocks):
         xb = xp_v[:, b * 128:(b + 1) * 128]
 
         def inject(ref):
-            flat_b = ref[b * gpb:(b + 1) * gpb].reshape(lanes, size).astype(BF16)
-            wide = jnp.dot(flat_b, spread, preferred_element_type=F32)
-            return nt_dot(xb, jnp.where(b_mask, wide, 0.0).astype(BF16))
+            mat = diagonal(ref[b * gpb:(b + 1) * gpb].reshape(128, state)).astype(BF16)
+            return jnp.dot(xb, mat, preferred_element_type=F32)
 
         zr_v[b] = inject(br_v)
         zi_v[b] = inject(bi_v)
@@ -150,7 +152,6 @@
     copies[6].wait()
     copies[7].wait()
     copies[8].wait()
-    c_mask = iota((128, lanes), 0) // size == iota((128, lanes), 1) // state
     for b in range(blocks):
         a1r, a1i = flat(t_r, b), flat(t_i, b)
         ar, ai = jnp.broadcast_to(a1r, (chunks, lanes)), jnp.broadcast_to(a1i, (chunks, lanes))
@@ -170,12 +171,8 @@
             gains_r.append(g_r)
             gains_i.append(g_i)
 
-        def diagonal(parts):
-            tall = jnp.concatenate(parts, axis=0)
-            wide = jnp.concatenate([tall] * gpb, axis=1)
-            return jnp.where(c_mask, wide, 0.0)
-
-        m_r, m_i = diagonal(gains_r), diagonal(gains_i)
+        m_r = diagonal(jnp.concatenate(gains_r, axis=0))
+        m_i = diagonal(jnp.concatenate(gains_i, axis=0))
         crm_v[b], cim_v[b] = m_r, m_i
         mats = jnp.concatenate([m_r.astype(BF16), (-m_i).astype(BF16)], axis=1)
         col = pl.ds(b * 128, 128)
@@ -251,6 +248,7 @@
     rows, channels = features.shape
     groups, state = lambda_real.shape
     size = input_real.shape[2]
+    input_real, input_imag = jnp.swapaxes(input_real, 1, 2), jnp.swapaxes(input_imag, 1, 2)
     width = value_weight.shape[1]
     gpb = 128 // size
     lanes, blocks, chunks = gpb * state, groups // gpb, 16
@@ -289,7 +287,7 @@
         out_specs=pl.BlockSpec(memory_space=pltpu.VMEM),
         scratch_shapes=scratch,
         compiler_params=pltpu.CompilerParams(
-            collective_id=0, has_side_effects=True, vmem_limit_bytes=60 * 1024 * 1024),
+            collective_id=0, has_side_effects=True, vmem_limit_bytes=32 * 1024 * 1024),
         name="mixer",
     )(*args)
 

time: 22.7 us -> 27.7 us (1.22)
  the two profiles are of different devices: /device:TPU:17 before, /device:TPU:9 now
where the time goes in v2:
time: 27.7 us; the launch traced here: 27.2 us
  Pallas kernels  14.3 us (52%)
  local copies, waits for them, and re-layouts  12.9 us (47%)
    pallas_call x1, Pallas kernels, local(): pl.pallas_call(functools.partial(kernel, nsp, ntp, (rows, groups, state,...  14.3 us
    unnamed x27, local copies, waits for them, and re-layouts  12.9 us

profile of v2, /device:TPU:9, one launch (start us, length us, event | category | flops | bytes accessed | tf_op | source)
XLA Modules:
  0.0 27.2 jit_solution(8629648869336277275)
XLA Ops:
  0.0 0.0 copy-start
  0.0 1.6 %copy-done = bf16[512,2048]{1,0:T(8,128)(2,1)S(1)} copy-done((bf16[512,2048]{1,0:T(8,128)(2,1)S(1)}, bf16[512,2048]{1,0:T(8,128)(2,1)}, u32[]{:S(2)}) %copy-start) | copy-done | bytes 2097176
  1.6 0.0 copy-start.1
  1.6 1.6 %copy-done.1 = bf16[512,2048]{1,0:T(8,128)(2,1)S(1)} copy-done((bf16[512,2048]{1,0:T(8,128)(2,1)S(1)}, bf16[512,2048]{1,0:T(8,128)(2,1)}, u32[]{:S(2)}) %copy-start.1) | copy-done | bytes 2097176
  3.2 0.0 copy-start.2
  3.2 0.9 %copy-done.2 = bf16[256,512]{1,0:T(8,128)(2,1)S(1)} copy-done((bf16[256,512]{1,0:T(8,128)(2,1)S(1)}, bf16[256,512]{1,0:T(8,128)(2,1)}, u32[]{:S(2)}) %copy-start.2) | copy-done | bytes 262168
  4.1 0.0 copy-start.3
  4.1 0.9 %copy-done.3 = f32[32,64,16]{1,2,0:T(8,128)S(1)} copy-done((f32[32,64,16]{1,2,0:T(8,128)S(1)}, f32[32,64,16]{1,2,0:T(8,128)}, u32[]{:S(2)}) %copy-start.3) | copy-done | bytes 131096
  5.1 0.0 copy-start.4
  5.1 0.9 %copy-done.4 = f32[32,64,16]{1,2,0:T(8,128)S(1)} copy-done((f32[32,64,16]{1,2,0:T(8,128)S(1)}, f32[32,64,16]{1,2,0:T(8,128)}, u32[]{:S(2)}) %copy-start.4) | copy-done | bytes 131096
  6.0 0.0 copy-start.5
  6.0 0.9 %copy-done.5 = f32[32,16,64]{2,1,0:T(8,128)S(1)} copy-done((f32[32,16,64]{2,1,0:T(8,128)S(1)}, f32[32,16,64]{2,1,0:T(8,128)}, u32[]{:S(2)}) %copy-start.5) | copy-done | bytes 131096
  7.0 0.0 copy-start.6
  7.0 0.9 %copy-done.6 = f32[32,16,64]{2,1,0:T(8,128)S(1)} copy-done((f32[32,16,64]{2,1,0:T(8,128)S(1)}, f32[32,16,64]{2,1,0:T(8,128)}, u32[]{:S(2)}) %copy-start.6) | copy-done | bytes 131096
  7.9 0.0 copy-start.7
  7.9 0.7 %copy-done.7 = f32[32,64]{1,0:T(8,128)S(1)} copy-done((f32[32,64]{1,0:T(8,128)S(1)}, f32[32,64]{1,0:T(8,128)}, u32[]{:S(2)}) %copy-start.7) | copy-done | bytes 8216
  8.7 0.0 copy-start.8
  8.7 0.7 %copy-done.8 = f32[32,64]{1,0:T(8,128)S(1)} copy-done((f32[32,64]{1,0:T(8,128)S(1)}, f32[32,64]{1,0:T(8,128)}, u32[]{:S(2)}) %copy-start.8) | copy-done | bytes 8216
  9.4 0.0 copy-start.9
  9.4 0.7 %copy-done.9 = f32[2048]{0:T(1024)S(1)} copy-done((f32[2048]{0:T(1024)S(1)}, f32[2048]{0:T(1024)}, u32[]{:S(2)}) %copy-start.9) | copy-done | bytes 8216
  10.1 0.0 copy-start.10
  10.1 0.7 %copy-done.10 = f32[2048]{0:T(1024)S(1)} copy-done((f32[2048]{0:T(1024)S(1)}, f32[2048]{0:T(1024)}, u32[]{:S(2)}) %copy-start.10) | copy-done | bytes 8216
  10.8 0.0 copy-start.11
  10.8 0.7 %copy-done.11 = f32[512]{0:T(512)S(1)} copy-done((f32[512]{0:T(512)S(1)}, f32[512]{0:T(512)}, u32[]{:S(2)}) %copy-start.11) | copy-done | bytes 2072
  11.4 0.0 copy-start.12
  11.5 0.7 %copy-done.12 = f32[32]{0:T(128)S(1)} copy-done((f32[32]{0:T(128)S(1)}, f32[32]{0:T(128)}, u32[]{:S(2)}) %copy-start.12) | copy-done | bytes 152
  12.1 14.3 %mixer.1 = bf16[128,2048]{1,0:T(8,128)(2,1)S(1)} custom-call(bf16[256,512]{1,0:T(8,128)(2,1)S(1)} %copy-done.2, f32[32,64]{1,0:T(8,128)S(1)} %copy-done.7, f32[32,64]{1,0:T(8,128)S(1)} %copy-done.8, f32[1,32]{1,0:T(1,128)S(1)} %bitcast.11, f32[32,16,64]{2,1,0:T(8,128)S(1)} %bitcast.6, f32[32,16,64]{2,1,0:T(8,128)S(1)} %bitcast.7, ...), custom_call_target="tpu_custom_call" | custom-call | tf_op jit(solution)/shard_map/mixer/pallas_call | solution.py:283
  26.4 0.8 %copy.15 = bf16[128,2048]{1,0:T(8,128)(2,1)} copy(bf16[128,2048]{1,0:T(8,128)(2,1)S(1)} %mixer.1) | data formatting | bytes 1048576
Async XLA Ops:
  0.0 1.6 %copy-start = (bf16[512,2048]{1,0:T(8,128)(2,1)S(1)}, bf16[512,2048]{1,0:T(8,128)(2,1)}, u32[]{:S(2)}) copy-start(bf16[512,2048]{1,0:T(8,128)(2,1)} %refs_9_.1) | copy-start | bytes 6291460
  1.6 1.6 %copy-start.1 = (bf16[512,2048]{1,0:T(8,128)(2,1)S(1)}, bf16[512,2048]{1,0:T(8,128)(2,1)}, u32[]{:S(2)}) copy-start(bf16[512,2048]{1,0:T(8,128)(2,1)} %refs_10_.1) | copy-start | bytes 6291460
  3.2 0.9 %copy-start.2 = (bf16[256,512]{1,0:T(8,128)(2,1)S(1)}, bf16[256,512]{1,0:T(8,128)(2,1)}, u32[]{:S(2)}) copy-start(bf16[256,512]{1,0:T(8,128)(2,1)} %refs_0_.1) | copy-start | bytes 786436
  4.1 0.9 %copy-start.3 = (f32[32,64,16]{1,2,0:T(8,128)S(1)}, f32[32,64,16]{1,2,0:T(8,128)}, u32[]{:S(2)}) copy-start(f32[32,64,16]{1,2,0:T(8,128)} %param.17) | copy-start | bytes 393220
  5.1 0.9 %copy-start.4 = (f32[32,64,16]{1,2,0:T(8,128)S(1)}, f32[32,64,16]{1,2,0:T(8,128)}, u32[]{:S(2)}) copy-start(f32[32,64,16]{1,2,0:T(8,128)} %param.18) | copy-start | bytes 393220
  6.0 0.9 %copy-start.5 = (f32[32,16,64]{2,1,0:T(8,128)S(1)}, f32[32,16,64]{2,1,0:T(8,128)}, u32[]{:S(2)}) copy-start(f32[32,16,64]{2,1,0:T(8,128)} %refs_6_.1) | copy-start | bytes 393220
  7.0 0.9 %copy-start.6 = (f32[32,16,64]{2,1,0:T(8,128)S(1)}, f32[32,16,64]{2,1,0:T(8,128)}, u32[]{:S(2)}) copy-start(f32[32,16,64]{2,1,0:T(8,128)} %refs_7_.1) | copy-start | bytes 393220
  7.9 0.7 %copy-start.7 = (f32[32,64]{1,0:T(8,128)S(1)}, f32[32,64]{1,0:T(8,128)}, u32[]{:S(2)}) copy-start(f32[32,64]{1,0:T(8,128)} %refs_1_.1) | copy-start | bytes 24580
  8.7 0.7 %copy-start.8 = (f32[32,64]{1,0:T(8,128)S(1)}, f32[32,64]{1,0:T(8,128)}, u32[]{:S(2)}) copy-start(f32[32,64]{1,0:T(8,128)} %refs_2_.1) | copy-start | bytes 24580
  9.4 0.7 %copy-start.9 = (f32[2048]{0:T(1024)S(1)}, f32[2048]{0:T(1024)}, u32[]{:S(2)}) copy-start(f32[2048]{0:T(1024)} %param.24) | copy-start | bytes 24580
  10.1 0.7 %copy-start.10 = (f32[2048]{0:T(1024)S(1)}, f32[2048]{0:T(1024)}, u32[]{:S(2)}) copy-start(f32[2048]{0:T(1024)} %param.25) | copy-start | bytes 24580
  10.8 0.7 %copy-start.11 = (f32[512]{0:T(512)S(1)}, f32[512]{0:T(512)}, u32[]{:S(2)}) copy-start(f32[512]{0:T(512)} %param.21) | copy-start | bytes 6148
  11.4 0.7 %copy-start.12 = (f32[32]{0:T(128)S(1)}, f32[32]{0:T(128)}, u32[]{:S(2)}) copy-start(f32[32]{0:T(128)} %param.16) | copy-start | bytes 388

commit v3 on v2

--- a/solution.py
+++ b/solution.py
@@ -282,12 +282,12 @@
     ]
     return pl.pallas_call(
         functools.partial(kernel, nsp, ntp, (rows, groups, state, size, width)),
-        out_shape=jax.ShapeDtypeStruct((rows // ntp, width), BF16),
+        out_shape=pltpu.VMEM((rows // ntp, width), BF16),
         in_specs=[pl.BlockSpec(memory_space=pl.ANY)] * len(args),
         out_specs=pl.BlockSpec(memory_space=pltpu.VMEM),
         scratch_shapes=scratch,
         compiler_params=pltpu.CompilerParams(
-            collective_id=0, has_side_effects=True, vmem_limit_bytes=32 * 1024 * 1024),
+            collective_id=0, has_side_effects=True, vmem_limit_bytes=60 * 1024 * 1024),
         name="mixer",
     )(*args)
 

time: 27.7 us -> 14.8 us (0.53); the launches traced: 27.2 us -> 14.7 us
  local copies, waits for them, and re-layouts: 12.9 us -> 0.8 us
  Pallas kernels: 14.3 us -> 13.9 us
    unnamed x27 -> x1, local copies, waits for them, and re-layouts: 12.9 us -> 0.8 us
    pallas_call x1, Pallas kernels: 14.3 us -> 13.9 us  [local(): pl.pallas_call(functools.partial(kernel, nsp, ntp, (rows, groups, state,...]
where the time goes in v3:
time: 14.8 us; the launch traced here: 14.7 us
  Pallas kernels  13.9 us (94%)
  local copies, waits for them, and re-layouts  0.8 us (5%)
    pallas_call x1, Pallas kernels, local(): pl.pallas_call(functools.partial(kernel, nsp, ntp, (rows, groups, state,...  13.9 us
    unnamed x1, local copies, waits for them, and re-layouts  0.8 us

profile of v3, /device:TPU:9, one launch (start us, length us, event | category | flops | bytes accessed | tf_op | source)
XLA Modules:
  0.0 14.7 jit_solution(13159061743636602443)
XLA Ops:
  0.0 13.9 %mixer.1 = bf16[128,2048]{1,0:T(8,128)(2,1)S(1)} custom-call(bf16[256,512]{1,0:T(8,128)(2,1)} %refs_0_.1, f32[32,64]{1,0:T(8,128)} %refs_1_.1, f32[32,64]{1,0:T(8,128)} %refs_2_.1, f32[1,32]{1,0:T(1,128)} %bitcast.11, f32[32,16,64]{2,1,0:T(8,128)} %bitcast.6, f32[32,16,64]{2,1,0:T(8,128)} %bitcast.7, f32[32,16,64]{2,1,0:T(8,128)} %refs_6_.1, ...), custom_call_target="tpu_custom_call" | custom-call | tf_op jit(solution)/shard_map/mixer/pallas_call | solution.py:283
  13.9 0.8 %copy.15 = bf16[128,2048]{1,0:T(8,128)(2,1)} copy(bf16[128,2048]{1,0:T(8,128)(2,1)S(1)} %mixer.1) | data formatting | bytes 1048576

commit v4 on v3

--- a/solution.py
+++ b/solution.py
@@ -43,7 +43,7 @@
     hbm = (ls_h, lr_h, li_h, x_h, br_h, bi_h, cr_h, ci_h, sk_h, vb_h, gb_h, vw_h, gw_h)
     vmem = (ls_v, lr_v, li_v, x_v, br_v, bi_v, cr_v, ci_v, sk_v, vb_v, gb_v, vw_v, gw_v)
     copies = [pltpu.make_async_copy(s, d, in_sem.at[i]) for i, (s, d) in enumerate(zip(hbm, vmem))]
-    for c in copies:
+    for c in copies[:6]:
         c.start()
 
     barrier = pltpu.get_barrier_semaphore()
@@ -90,6 +90,8 @@
 
     copies[4].wait()
     copies[5].wait()
+    for c in copies[6:]:
+        c.start()
     crow = iota((chunks, lanes), 0)
 
     def shift(value, s):
@@ -147,7 +149,7 @@
 
     @pl.loop(me + 1, nsp)
     def _(d):
-        outgoing(nsp + me - d).start()
+        outgoing(d).start()
 
     copies[6].wait()
     copies[7].wait()
@@ -181,15 +183,17 @@
     A_r, A_i = a_all_v[:blocks], a_all_v[blocks:]
     zero = jnp.zeros((blocks, lanes), F32)
 
-    def horner(d, h):
+    def gather(k, carry):
+        h_r, h_i, p_r, p_i = carry
+        d = me - 1 - k
         pltpu.make_async_remote_copy(
             src_ref=msg_v, dst_ref=recv_v.at[d], send_sem=send_sem.at[d], recv_sem=recv_sem.at[d],
             device_id=(d, core), device_id_type=MESH).wait_recv()
         got = recv_v[d].astype(F32)
-        n_r, n_i = cmul(A_r, A_i, h[0], h[1])
-        return n_r + got[:blocks], n_i + got[blocks:]
-
-    h_r, h_i = lax.fori_loop(0, me, horner, (zero, zero))
+        m_r, m_i = cmul(p_r, p_i, got[:blocks], got[blocks:])
+        return (h_r + m_r, h_i + m_i) + cmul(p_r, p_i, A_r, A_i)
+
+    h_r, h_i, _, _ = lax.fori_loop(0, me, gather, (zero, zero, zero + 1.0, zero))
     h_v[:blocks] = h_r
     h_v[blocks:] = h_i
 
@@ -240,7 +244,7 @@
 
     @pl.loop(me + 1, nsp)
     def _(d):
-        outgoing(nsp + me - d).wait_send()
+        outgoing(d).wait_send()
 
 
 def local(nsp, ntp, features, lambda_real, lambda_imag, log_step, input_real, input_imag, real_output,

time: 14.8 us -> 14.6 us (0.986)
  the two profiles are of different devices: /device:TPU:9 before, /device:TPU:29 now
where the time goes in v4:
time: 14.6 us; the launch traced here: 14.5 us
  Pallas kernels  13.7 us (94%)
  local copies, waits for them, and re-layouts  0.8 us (5%)
    pallas_call x1, Pallas kernels, local(): pl.pallas_call(functools.partial(kernel, nsp, ntp, (rows, groups, state,...  13.7 us
    unnamed x1, local copies, waits for them, and re-layouts  0.8 us

profile of v4, /device:TPU:29, one launch (start us, length us, event | category | flops | bytes accessed | tf_op | source)
XLA Modules:
  0.0 14.5 jit_solution(14678906565939265567)
XLA Ops:
  0.0 13.7 %mixer.1 = bf16[128,2048]{1,0:T(8,128)(2,1)S(1)} custom-call(bf16[256,512]{1,0:T(8,128)(2,1)} %refs_0_.1, f32[32,64]{1,0:T(8,128)} %refs_1_.1, f32[32,64]{1,0:T(8,128)} %refs_2_.1, f32[1,32]{1,0:T(1,128)} %bitcast.11, f32[32,16,64]{2,1,0:T(8,128)} %bitcast.6, f32[32,16,64]{2,1,0:T(8,128)} %bitcast.7, f32[32,16,64]{2,1,0:T(8,128)} %refs_6_.1, ...), custom_call_target="tpu_custom_call" | custom-call | tf_op jit(solution)/shard_map/mixer/pallas_call | solution.py:287
  13.7 0.8 %copy.15 = bf16[128,2048]{1,0:T(8,128)(2,1)} copy(bf16[128,2048]{1,0:T(8,128)(2,1)S(1)} %mixer.1) | data formatting | bytes 1048576
